TPU v7x, 32 devices: a whole 2x2x4 slice. The times are simulated.
32 devices in a mesh: grp: 2 (over x), ep: 8 (over z, y), tp: 2 (over core).
Axes of the slice: x: 2, y: 2, z: 4, core: 2. Of those that a mesh axis runs over, the one named last changes fastest.
Arguments:
- tokens: bfloat16 [1024, 2048], P(('grp', 'ep')), parts along dimension 0, may hold values from -6 to 6
- norm_gain: float32 [2048], replicated, may hold values from 0.1 to 1.9
- groups: int32 [1024], P(('grp', 'ep')), parts along dimension 0, may hold values from 0 to 1, as said below
- picks: int32 [1024, 4], P(('grp', 'ep')), parts along dimension 0, may hold values from 0 to 7, as said below
- gates: float32 [1024, 4], P(('grp', 'ep')), parts along dimension 0, may hold values from 0.1 to 1
- w_gate: bfloat16 [16, 2048, 512], P('ep', None, 'tp'), may hold values from -0.125 to 0.125
- w_up: bfloat16 [16, 2048, 512], P('ep', None, 'tp'), may hold values from -0.125 to 0.125
- w_down: bfloat16 [16, 512, 2048], P('ep', 'tp'), may hold values from -0.25 to 0.25
Outputs:
- mixed: bfloat16 [1024, 2048], P(('grp', 'ep'), 'tp'), parts along dimension 0
There are 2 independent parts, one for each index of `grp`. A program takes and returns all parts, laid end to end along the dimension named above; an argument that names none is the same for every part. Nothing has to cross between parts.
Inputs may be any that keep to these rules, and one draw needn't show every extreme that they name: `groups`: among the tokens of one device, exactly 32 lie in one common group and all of them name one common expert of it as their first pick; every other token of that device lies in another group. A token's 4 picks are distinct. Among the tokens of one device at most 32 name any one expert (group and pick together), and in every draw one expert is named by exactly 32 tokens of every device.
All inputs are finite; a program needn't handle non-finite values.
Results may differ from a plain program's by a relative error of at most 0.014.
Values may be sent and summed in bfloat16 or wider, within the bound.
A program may use at most 64 MiB of HBM per device.

v0:
```python
import functools
import math

import jax
import jax.numpy as jnp
from jax import lax
from jax.experimental import pallas as pl
from jax.experimental.pallas import tpu as pltpu
from jax.sharding import PartitionSpec as P

GROUPS = 2
MESH = pl.DeviceIdType.MESH
EPS = 1e-06
EXT = 128
PIECES = 2
VMEM_LIMIT = 66879488
F32 = jnp.float32
BF16 = jnp.bfloat16


def kernel(
    dims,
    tok_hbm,
    gain_hbm,
    grp_hbm,
    pick_hbm,
    gate_hbm,
    wg_hbm,
    wu_hbm,
    wd_hbm,
    out_ref,
    tok_ref,
    gain_ref,
    grp_ref,
    pick_ref,
    gate_ref,
    wg,
    wu,
    wd,
    xbuf,
    cross_out,
    psend,
    precv,
    ymine,
    rsend,
    rrecv,
    csend,
    crecv,
    w_sem,
    x_send,
    x_recv,
    d_send,
    d_recv,
    p_send,
    p_recv,
    r_send,
    r_recv,
    c_send,
    c_recv,
):
    members, gcap, local, top, width, chunk = dims
    tokens = tok_ref.shape[0]
    half = gcap // 2
    cols = width // 2
    pcols = cols // PIECES
    full = width + EXT
    cuts = [width // PIECES * p for p in range(PIECES)] + [full]
    ep = lax.axis_index("ep")
    c = lax.axis_index("tp")
    g = ep // members
    m = ep % members
    cross_ep = (1 - g) * members + m
    rows_c = pl.ds(pl.multiple_of(c * half, half), half)

    def member(i):
        return {"ep": g * members + i, "tp": c}

    mate = {"ep": ep, "tp": 1 - c}
    cross = {"ep": cross_ep, "tp": c}

    barrier = pltpu.get_barrier_semaphore()
    peers = [member((m + d) % members) for d in range(1, members)] + [mate, cross]
    for peer in peers:
        pl.semaphore_signal(barrier, inc=1, device_id=peer, device_id_type=MESH)
    pairs = (
        (grp_hbm, grp_ref),
        (pick_hbm, pick_ref),
        (gate_hbm, gate_ref),
        (gain_hbm, gain_ref),
        (tok_hbm, tok_ref),
        (wg_hbm, wg),
        (wu_hbm, wu),
        (wd_hbm, wd),
    )
    loads = [
        pltpu.make_async_copy(src, dst, w_sem.at[i]) for i, (src, dst) in enumerate(pairs)
    ]
    for load in loads:
        load.start()
    for load in loads[:3]:
        load.wait()

    mine_row = jnp.broadcast_to(grp_ref[...] == g, (8, tokens)).astype(F32)
    tri = (
        lax.broadcasted_iota(jnp.int32, (tokens, tokens), 0)
        < lax.broadcasted_iota(jnp.int32, (tokens, tokens), 1)
    ).astype(F32)
    rank = jnp.dot(mine_row, tri, preferred_element_type=F32)[0:1, :]
    mine = mine_row[0:1, :]
    col = lax.broadcasted_iota(jnp.int32, (1, tokens), 1).astype(F32)
    slot_row = lax.broadcasted_iota(jnp.int32, (gcap, tokens), 0).astype(F32)
    sel_own = jnp.where(slot_row == rank, mine, 0.0)
    sel_oth = jnp.where(slot_row == col - rank, 1.0 - mine, 0.0)
    half_row = (lax.broadcasted_iota(jnp.int32, (half, tokens), 0) + c * half).astype(F32)
    sel_oth_half = jnp.where(half_row == col - rank, 1.0 - mine, 0.0)

    line = lax.broadcasted_iota(jnp.int32, (EXT, tokens), 0)
    spread = jnp.zeros((EXT, tokens), F32)
    for j in range(top):
        spread += jnp.where(pick_ref[j : j + 1, :] == line % (EXT // 2), gate_ref[j : j + 1, :], 0.0)
    high = spread.astype(BF16).astype(F32)
    ext = jnp.where(line < EXT // 2, high, spread - high).astype(BF16)
    pick_half = sel_oth_half.astype(BF16)
    pick_own = sel_own.astype(BF16)
    last = (((1,), (1,)), ((), ()))
    cross_out[:, width:] = lax.dot_general(
        pick_half, ext, last, preferred_element_type=F32
    ).astype(BF16)
    for load in loads[3:5]:
        load.wait()
    values = tok_ref[...].astype(F32)
    scale = lax.rsqrt(jnp.mean(values * values, axis=-1, keepdims=True) + EPS)
    normed = (values * scale * gain_ref[...]).astype(BF16)
    cross_out[:, :width] = jnp.dot(pick_half, normed, preferred_element_type=F32).astype(BF16)

    pl.semaphore_wait(barrier, len(peers))
    def span(p):
        return pl.ds(cuts[p], cuts[p + 1] - cuts[p])

    sends = []
    for p in range(PIECES):
        copy = pltpu.make_async_remote_copy(
            src_ref=cross_out.at[:, span(p)],
            dst_ref=xbuf.at[members + m, rows_c, span(p)],
            send_sem=c_send.at[0, p],
            recv_sem=x_recv.at[members + m, p],
            device_id=cross,
            device_id_type=MESH,
        )
        copy.start()
        sends.append(copy)

    xbuf[m, :, width:] = lax.dot_general(
        pick_own, ext, last, preferred_element_type=F32
    ).astype(BF16)
    xbuf[m, :, :width] = jnp.dot(pick_own, normed, preferred_element_type=F32).astype(BF16)

    def x_copy(slot, p, dest, sem):
        return pltpu.make_async_remote_copy(
            src_ref=xbuf.at[slot, rows_c, span(p)],
            dst_ref=xbuf.at[slot, rows_c, span(p)],
            send_sem=x_send.at[sem, p],
            recv_sem=x_recv.at[slot, p],
            device_id=dest,
            device_id_type=MESH,
        )

    def d_copy(slot, p, which):
        rows = pl.ds(pl.multiple_of(which * half, half), half)
        return pltpu.make_async_remote_copy(
            src_ref=xbuf.at[slot, rows, span(p)],
            dst_ref=xbuf.at[slot, rows, span(p)],
            send_sem=d_send.at[slot, p],
            recv_sem=d_recv.at[slot, p],
            device_id=mate,
            device_id_type=MESH,
        )

    def start(copy):
        copy.start()
        sends.append(copy)

    for p in range(PIECES):
        for d in range(1, members):
            start(x_copy(m, p, member((m + d) % members), d))
    for p in range(PIECES):
        for d in range(1, members):
            slot = (m + members - d) % members
            x_copy(slot, p, mate, 0).wait_recv()
            start(d_copy(slot, p, c))
    for p in range(PIECES):
        x_copy(members + m, p, mate, 0).wait_recv()
        for d in range(1, members):
            start(x_copy(members + m, p, member((m + d) % members), members + d))
        start(d_copy(members + m, p, c))
    for p in range(PIECES):
        for d in range(1, members):
            d_copy((m + members - d) % members, p, 1 - c).wait_recv()
    for load in loads[5:]:
        load.wait()

    per = chunk // gcap
    lane_x = lax.broadcasted_iota(jnp.int32, (chunk, EXT), 1)
    steps = members * gcap // chunk
    kcut = width // PIECES

    def chunk_rows(i):
        return pl.ds(i * chunk, chunk)

    def wide(core, p):
        return pl.ds(pl.multiple_of(core * cols + p * pcols, pcols), pcols)

    def compute(part, ready):
        def body(i, wait):
            blocks = pl.ds(part * members + i * per, per)
            gate_pre = [jnp.zeros((chunk, wg.shape[2]), F32) for _ in range(local)]
            up_pre = [jnp.zeros((chunk, wg.shape[2]), F32) for _ in range(local)]
            for p in range(PIECES):
                wait(p)
                k = pl.ds(p * kcut, kcut)
                rows = xbuf[blocks, :, k].reshape(chunk, kcut)
                for j in range(local):
                    gate_pre[j] += jnp.dot(rows, wg[j, k], preferred_element_type=F32)
                    up_pre[j] += jnp.dot(rows, wu[j, k], preferred_element_type=F32)
            tail = xbuf[blocks, :, width:].reshape(chunk, EXT).astype(F32)
            hidden = []
            for j in range(local):
                weight = jnp.sum(
                    jnp.where(lane_x % (EXT // 2) == m * local + j, tail, 0.0),
                    axis=1,
                    keepdims=True,
                )
                act = gate_pre[j] / (1.0 + jnp.exp(-gate_pre[j])) * up_pre[j]
                hidden.append((act * weight).astype(BF16))

            def down(core, p):
                total = jnp.zeros((chunk, pcols), F32)
                for j in range(local):
                    total += jnp.dot(hidden[j], wd[j, :, wide(core, p)], preferred_element_type=F32)
                return total

            for p in range(PIECES):
                psend[part, p, chunk_rows(i)] = down(1 - c, p).astype(BF16)
                p_copy(part, p, i).start()
            for p in range(PIECES):
                ymine[part, p, chunk_rows(i)] = down(c, p)

        if steps == 1:
            body(0, ready)
        else:
            for p in range(PIECES):
                ready(p)

            def loop(i, carry):
                body(i, lambda p: None)
                return carry

            lax.fori_loop(0, steps, loop, 0)

    def p_copy(part, p, i):
        return pltpu.make_async_remote_copy(
            src_ref=psend.at[part, p, chunk_rows(i)],
            dst_ref=precv.at[part, p, chunk_rows(i)],
            send_sem=p_send.at[part, p, i],
            recv_sem=p_recv.at[part, p, i],
            device_id=mate,
            device_id_type=MESH,
        )

    def r_copy(part, p, to_slot, from_slot, dest, sem):
        return pltpu.make_async_remote_copy(
            src_ref=rsend.at[part, p, to_slot],
            dst_ref=rrecv.at[part, p, from_slot],
            send_sem=r_send.at[part, p, sem],
            recv_sem=r_recv.at[part, p, from_slot],
            device_id=dest,
            device_id_type=MESH,
        )

    def reduce_tp(part):
        for p in range(PIECES):

            def body(i, carry):
                p_copy(part, p, i).wait()
                total = ymine[part, p, chunk_rows(i)] + precv[part, p, chunk_rows(i)].astype(F32)
                rsend[part, p, pl.ds(i * per, per)] = total.astype(BF16).reshape(per, gcap, pcols)
                return carry

            if steps == 1:
                body(0, 0)
            else:
                lax.fori_loop(0, steps, body, 0)
            for d in range(1, members):
                dest = (m + d) % members
                start(r_copy(part, p, dest, m, member(dest), d))

    def collect(part, p):
        total = rsend[part, p, m].astype(F32)
        for d in range(1, members):
            slot = (m + members - d) % members
            r_copy(part, p, slot, slot, mate, 0).wait_recv()
            total += rrecv[part, p, slot].astype(F32)
        return total.astype(BF16)

    def relayed(p):
        for d in range(1, members):
            slot = members + (m + members - d) % members
            x_copy(slot, p, mate, 0).wait_recv()
            start(d_copy(slot, p, c))

    def crossed(p):
        for d in range(members):
            d_copy(members + (m + members - d) % members, p, 1 - c).wait_recv()

    compute(0, lambda p: None)
    for p in range(PIECES):
        relayed(p)
    reduce_tp(0)
    compute(1, crossed)
    reduce_tp(1)
    own = [collect(0, p) for p in range(PIECES)]
    back = []
    for p in range(PIECES):
        csend[p] = collect(1, p)
        copy = pltpu.make_async_remote_copy(
            src_ref=csend.at[p],
            dst_ref=crecv.at[p],
            send_sem=c_send.at[1, p],
            recv_sem=c_recv.at[p],
            device_id=cross,
            device_id_type=MESH,
        )
        copy.start()
        back.append(copy)
    turn = (((0,), (0,)), ((), ()))
    pick_oth = sel_oth.astype(BF16)
    mixed = [lax.dot_general(pick_own, own[p], turn, preferred_element_type=F32) for p in range(PIECES)]
    for copy in sends:
        copy.wait_send()
    for p in range(PIECES):
        back[p].wait()
        total = mixed[p] + lax.dot_general(pick_oth, crecv[p], turn, preferred_element_type=F32)
        out_ref[:, p * pcols : (p + 1) * pcols] = total.astype(BF16)


def on_device(tokens, norm_gain, groups, picks, gates, w_gate, w_up, w_down):
    tok_rows, width = tokens.shape
    top = picks.shape[1]
    local, _, ff = w_gate.shape
    senders = lax.axis_size("ep")
    members = senders // GROUPS
    hot = tok_rows * top // (senders * local // GROUPS)
    gcap = -(-max(hot, tok_rows - hot) // 32) * 32
    assert members * local <= EXT // 2
    chunk = max(gcap, min(128, members * gcap))
    steps = members * gcap // chunk
    pcols = width // 2 // PIECES
    full = width + EXT
    dims = (members, gcap, local, top, width, chunk)
    vmem = pl.BlockSpec(memory_space=pltpu.VMEM)
    hbm = pl.BlockSpec(memory_space=pl.ANY)
    dma = pltpu.SemaphoreType.DMA
    buffers = [
        ((tok_rows, width), BF16),
        ((1, width), F32),
        ((1, tok_rows), jnp.int32),
        ((top, tok_rows), jnp.int32),
        ((top, tok_rows), F32),
        ((local, width, ff), BF16),
        ((local, width, ff), BF16),
        ((local, ff, width), BF16),
        ((2 * members, gcap, full), BF16),
        ((gcap // 2, full), BF16),
        ((2, PIECES, members * gcap, pcols), BF16),
        ((2, PIECES, members * gcap, pcols), BF16),
        ((2, PIECES, members * gcap, pcols), F32),
        ((2, PIECES, members, gcap, pcols), BF16),
        ((2, PIECES, members, gcap, pcols), BF16),
        ((PIECES, gcap, pcols), BF16),
        ((PIECES, gcap, pcols), BF16),
    ]
    size = sum(math.prod(shape) * jnp.dtype(kind).itemsize for shape, kind in buffers)
    return pl.pallas_call(
        functools.partial(kernel, dims),
        out_shape=jax.ShapeDtypeStruct((tok_rows, width // 2), BF16),
        in_specs=[hbm] * 8,
        out_specs=vmem,
        scratch_shapes=[pltpu.VMEM(shape, kind) for shape, kind in buffers]
        + [
            dma((8,)),
            dma((2 * members, PIECES)),
            dma((2 * members, PIECES)),
            dma((2 * members, PIECES)),
            dma((2 * members, PIECES)),
            dma((2, PIECES, steps)),
            dma((2, PIECES, steps)),
            dma((2, PIECES, members)),
            dma((2, PIECES, members)),
            dma((2, PIECES)),
            dma((PIECES,)),
        ],
        compiler_params=pltpu.CompilerParams(
            collective_id=0, has_side_effects=True, vmem_limit_bytes=VMEM_LIMIT or size + 8 * 2**20
        ),
    )(
        tokens,
        norm_gain.reshape(1, width),
        groups.reshape(1, tok_rows),
        picks.T,
        gates.T,
        w_gate,
        w_up,
        w_down,
    )


def solution(mesh):
    in_specs = (
        P(("grp", "ep"), None),
        P(),
        P(("grp", "ep")),
        P(("grp", "ep"), None),
        P(("grp", "ep"), None),
        P("ep", None, "tp"),
        P("ep", None, "tp"),
        P("ep", "tp", None),
    )
    out_specs = P(("grp", "ep"), "tp")
    return jax.shard_map(
        on_device, mesh=mesh, in_specs=in_specs, out_specs=out_specs, check_vma=False
    )
```

profile of v0, /device:TPU:0, one launch (start us, length us, event | category | flops | bytes accessed | tf_op | source)
XLA Modules:
  0.0 30.4 jit_solution(582317584559778750)
XLA Ops:
  0.0 28.9 %shard_map.82 = bf16[64,1024]{1,0:T(8,128)(2,1)} custom-call(bf16[64,2048]{1,0:T(8,128)(2,1)} %tok_hbm.1, f32[1,2048]{1,0:T(1,128)} %bitcast.4, s32[1,64]{1,0:T(1,128)} %bitcast.7, s32[4,64]{1,0:T(4,128)} %bitcast.5, f32[4,64]{1,0:T(4,128)} %bitcast.6, bf16[2,2048,256]{2,1,0:T(8,128)(2,1)} %wg_hbm.1, bf16[2,2048,256]{2,1,0:T(8,128)(2,1)} %wu_hbm.1, ...), custom_call_target="tpu_custom_call" | custom-call | tf_op jit(solution)/shard_map/pallas_call | solution.py:383
  28.9 1.6 %copy.10 = bf16[64,1024]{1,0:T(8,128)(2,1)} copy(bf16[64,1024]{1,0:T(8,128)(2,1)} %shard_map.82) | data formatting | bytes 262144
where the time goes:
time: 30.6 us; the launch traced here: 30.4 us
  Pallas kernels  28.9 us (94%)
  local copies, waits for them, and re-layouts  1.57 us (5%)
    pallas_call x1, Pallas kernels, on_device(): pl.pallas_call(functools.partial(kernel, dims), out_shape=jax.ShapeDtypeS...  28.9 us
    unnamed x1, local copies, waits for them, and re-layouts  1.57 us

commit v1 on v0

--- a/solution.py
+++ b/solution.py
@@ -13,7 +13,6 @@
 EPS = 1e-06
 EXT = 128
 PIECES = 2
-VMEM_LIMIT = 66879488
 F32 = jnp.float32
 BF16 = jnp.bfloat16
 
@@ -400,17 +399,22 @@
             dma((PIECES,)),
         ],
         compiler_params=pltpu.CompilerParams(
-            collective_id=0, has_side_effects=True, vmem_limit_bytes=VMEM_LIMIT or size + 8 * 2**20
+            collective_id=0, has_side_effects=True, vmem_limit_bytes=size + 8 * 2**20
         ),
     )(
-        tokens,
-        norm_gain.reshape(1, width),
-        groups.reshape(1, tok_rows),
-        picks.T,
-        gates.T,
-        w_gate,
-        w_up,
-        w_down,
+        *(
+            pltpu.with_memory_space_constraint(x, pltpu.HBM)
+            for x in (
+                tokens,
+                norm_gain.reshape(1, width),
+                groups.reshape(1, tok_rows),
+                picks.T,
+                gates.T,
+                w_gate,
+                w_up,
+                w_down,
+            )
+        )
     )
 
 

time: 30.6 us -> 29 us (0.948)
  local copies, waits for them, and re-layouts: 1.57 us -> 0.66 us
  Pallas kernels: 28.9 us -> 28.2 us
    unnamed x1, local copies, waits for them, and re-layouts: 1.57 us -> 0.66 us
    pallas_call x1, Pallas kernels: 28.9 us -> 28.2 us  [on_device(): pl.pallas_call(functools.partial(kernel, dims), out_shape=jax.ShapeDtypeS...]
where the time goes in v1:
time: 29 us; the launch traced here: 28.9 us
  Pallas kernels  28.2 us (97%)
  local copies, waits for them, and re-layouts  0.66 us (2%)
    pallas_call x1, Pallas kernels, on_device(): pl.pallas_call(functools.partial(kernel, dims), out_shape=jax.ShapeDtypeS...  28.2 us
    unnamed x1, local copies, waits for them, and re-layouts  0.66 us

profile of v1, /device:TPU:0, one launch (start us, length us, event | category | flops | bytes accessed | tf_op | source)
XLA Modules:
  0.0 28.9 jit_solution(15382523051949274516)
XLA Ops:
  0.0 28.2 %shard_map.82 = bf16[64,1024]{1,0:T(8,128)(2,1)S(1)} custom-call(bf16[64,2048]{1,0:T(8,128)(2,1)} %tok_hbm.1, f32[1,2048]{1,0:T(1,128)} %bitcast.4, s32[1,64]{1,0:T(1,128)} %bitcast.7, s32[4,64]{1,0:T(4,128)} %bitcast.5, f32[4,64]{1,0:T(4,128)} %bitcast.6, bf16[2,2048,256]{2,1,0:T(8,128)(2,1)} %wg_hbm.1, bf16[2,2048,256]{2,1,0:T(8,128)(2,1)} %wu_hbm.1, ...), custom_call_target="tpu_custom_call" | custom-call | tf_op jit(solution)/shard_map/pallas_call | solution.py:382
  28.2 0.7 %copy.10 = bf16[64,1024]{1,0:T(8,128)(2,1)} copy(bf16[64,1024]{1,0:T(8,128)(2,1)S(1)} %shard_map.82) | data formatting | bytes 262144
